TPU v7x, 32 devices: a whole 2x2x4 slice. The times are simulated.
32 devices in a mesh: fs: 8 (over z, y), tp: 4 (over x, core).
Axes of the slice: x: 2, y: 2, z: 4, core: 2. Of those that a mesh axis runs over, the one named last changes fastest.
Arguments:
- tokens: bfloat16 [8192, 2048], P('fs', 'tp'), may hold values from -6 to 6
- norm_gain: float32 [2048], P('fs'), may hold values from 0.1 to 1.9
- up_master: float32 [2048, 4096], P('fs', 'tp'), may hold values from -0.125 to 0.125
- down_master: float32 [4096, 2048], P('fs', 'tp'), may hold values from -0.09375 to 0.09375
Outputs:
- mixed: bfloat16 [8192, 2048], P('fs', 'tp')
- up_ready: bfloat16 [2048, 4096], P(None, 'tp')
- down_ready: bfloat16 [4096, 2048], P('tp')
All inputs are finite; a program needn't handle non-finite values.
Results may differ from a plain program's by a relative error of at most 0.0095.
Values may be sent and summed in bfloat16 or wider, within the bound.
A program may use at most 128 MiB of HBM per device.

v0:
```python
import jax
import jax.numpy as jnp
from jax import lax
from jax.sharding import PartitionSpec as P


def shards(tokens, norm_gain, up_master, down_master):
    up_local = (norm_gain[:, None] * up_master).astype(jnp.bfloat16)
    up_ready = lax.all_gather(up_local, "fs", axis=0, tiled=True)
    down_local = down_master.astype(jnp.bfloat16)
    gathered = lax.all_gather(down_local, "fs", axis=0, tiled=True)
    down_ready = lax.all_to_all(gathered, "tp", split_axis=0, concat_axis=1, tiled=True)
    features = lax.all_gather(tokens, "tp", axis=1, tiled=True)
    values = features.astype(jnp.float32)
    mean_square = jnp.mean(values * values, axis=-1, keepdims=True)
    normed = (values * lax.rsqrt(mean_square + 1e-06)).astype(jnp.bfloat16)
    before = jnp.dot(normed, up_ready, preferred_element_type=jnp.float32)
    hidden = jnp.square(jax.nn.relu(before)).astype(jnp.bfloat16)
    partial_value = jnp.dot(hidden, down_ready, preferred_element_type=jnp.float32)
    mixed = lax.psum_scatter(
        partial_value.astype(jnp.bfloat16), "tp", scatter_dimension=1, tiled=True
    )
    return (mixed, up_ready, down_ready)


def solution(mesh):
    return jax.shard_map(
        shards,
        mesh=mesh,
        in_specs=(P("fs", "tp"), P("fs"), P("fs", "tp"), P("fs", "tp")),
        out_specs=(P("fs", "tp"), P(None, "tp"), P("tp", None)),
        check_vma=False,
    )
```

profile of v0, /device:TPU:0, one launch (start us, length us, event | category | flops | bytes accessed | tf_op | source)
XLA Modules:
  0.0 287.9 jit_solution(17428654618168584598)
XLA Ops:
  7.2 0.0 all-gather.8.cloned.1.call-start
  7.2 2.1 convert_element_type.22
  9.3 0.0 all-gather.8.cloned.1.call-update
  9.3 0.0 all-gather.4.cloned.1.call-start
  9.4 0.7 all-gather.4.cloned.1.call-update
  10.1 0.0 all-gather.6.cloned.1.call-start
  10.1 2.1 multiply_convert_fusion.2
  12.3 0.0 all-gather.6.cloned.1.call-update
  12.3 73.9 %all-gather.8.cloned.1.call-done = bf16[4096,512]{1,0:T(8,128)(2,1)} async-done(((bf16[512,512]{1,0:T(8,128)(2,1)}), bf16[4096,512]{1,0:T(8,128)(2,1)}) %all-gather.8.cloned.1.call-update) | async-done | bytes 4194320 | tf_op jit(solution)/shard_map/all_gather | solution.py:11
  86.2 4.9 %all-to-all-start = ((bf16[4,1024,512]{2,1,0:T(8,128)(2,1)}), bf16[4,1024,512]{2,1,0:T(8,128)(2,1)}, u32[]{:S(2)}, u32[]{:S(2)}) async-start(bf16[4,1024,512]{2,1,0:T(8,128)(2,1)} %bitcast.8), calls=%async_computation | async-start | bytes 8388608 | tf_op jit(solution)/shard_map/all_to_all | solution.py:12
  91.1 0.0 reduce-scatter.2.cloned.1.call-start
  91.2 52.2 %all-gather.4.cloned.1.call-done = bf16[1024,2048]{1,0:T(8,128)(2,1)} async-done(((bf16[1024,512]{1,0:T(8,128)(2,1)}), bf16[1024,2048]{1,0:T(8,128)(2,1)}) %all-gather.4.cloned.1.call-update) | async-done | bytes 4194320 | tf_op jit(solution)/shard_map/all_gather | solution.py:13
  143.4 3.1 %fusion = f32[1024]{0:T(1024)S(1)} fusion(bf16[1024,2048]{1,0:T(8,128)(2,1)} %all-gather.4.cloned.1.call-done), kind=kLoop, calls=%fused_computation.2 | loop fusion | flops 6290432 | bytes 4198400 | tf_op jit(solution)/shard_map/reduce_sum | solution.py:15
  146.5 15.3 %all-to-all-done = bf16[4,1024,512]{2,1,0:T(8,128)(2,1)} async-done(((bf16[4,1024,512]{2,1,0:T(8,128)(2,1)}), bf16[4,1024,512]{2,1,0:T(8,128)(2,1)}, u32[]{:S(2)}, u32[]{:S(2)}) %all-to-all-start) | async-done | bytes 4194336 | tf_op jit(solution)/shard_map/all_to_all | solution.py:12
  161.8 6.2 %copy.8 = bf16[4,1024,512]{1,2,0:T(8,128)(2,1)} copy(bf16[4,1024,512]{2,1,0:T(8,128)(2,1)} %all-to-all-done) | data formatting | bytes 8388608 | tf_op jit(solution)/shard_map/all_to_all | solution.py:12
  168.0 50.9 %all-gather.6.cloned.1.call-done = bf16[2048,1024]{1,0:T(8,128)(2,1)} async-done(((bf16[256,1024]{1,0:T(8,128)(2,1)}), bf16[2048,1024]{1,0:T(8,128)(2,1)}) %all-gather.6.cloned.1.call-update) | async-done | bytes 4194320 | tf_op jit(solution)/shard_map/all_gather | solution.py:9
  218.9 14.7 %convolution_convert_fusion = bf16[1024,2048]{1,0:T(8,128)(2,1)} fusion(bf16[1024,2048]{0,1:T(8,128)(2,1)} %bitcast.6, bf16[2048,1024]{1,0:T(8,128)(2,1)} %all-gather.6.cloned.1.call-done, bf16[1024,2048]{1,0:T(8,128)(2,1)} %all-gather.4.cloned.1.call-done, f32[1024]{0:T(1024)S(1)} %add_rsqrt_fusion), kind=kOutput, calls=%fused_computation.7 | convolution fusion | flops 8601468928 | bytes 16781312 | tf_op jit(solution)/shard_map/dot_general | solution.py:19
  233.6 0.0 reduce-scatter.2.cloned.1.call-update
  233.6 6.5 %copy.9 = bf16[1024,2048]{1,0:T(8,128)(2,1)} copy(bf16[1024,2048]{0,1:T(8,128)(2,1)} %bitcast.7) | data formatting | bytes 8388608
  240.1 36.6 %reduce-scatter.2.cloned.1.call-done = bf16[1024,512]{1,0:T(8,128)(2,1)} async-done(((bf16[1024,2048]{1,0:T(8,128)(2,1)}), bf16[1024,512]{1,0:T(8,128)(2,1)}) %reduce-scatter.2.cloned.1.call-update) | async-done | bytes 1048592 | tf_op jit(solution)/shard_map/reduce_scatter | solution.py:20
  276.7 4.6 %copy.11 = bf16[2048,1024]{1,0:T(8,128)(2,1)} copy(bf16[2048,1024]{1,0:T(8,128)(2,1)} %all-gather.6.cloned.1.call-done) | data formatting | bytes 8388608
  (1 shorter events, 0.0 us)
Async XLA Ops:
  7.2 79.1 %all-gather.8.cloned.1.call-start = ((), (), s32[]{:S(2)}) async-start(), calls=%async_computation.4 | async-start | bytes 4718592 | tf_op jit(solution)/shard_map/all_gather | solution.py:11
  9.3 134.1 %all-gather.4.cloned.1.call-start = ((), (), s32[]{:S(2)}) async-start(), calls=%async_computation.2 | async-start | bytes 5242880 | tf_op jit(solution)/shard_map/all_gather | solution.py:13
  10.1 208.8 %all-gather.6.cloned.1.call-start = ((), (), s32[]{:S(2)}) async-start(), calls=%async_computation.3 | async-start | bytes 4718592 | tf_op jit(solution)/shard_map/all_gather | solution.py:9
  86.2 75.6 %all-to-all-start = ((bf16[4,1024,512]{2,1,0:T(8,128)(2,1)}), bf16[4,1024,512]{2,1,0:T(8,128)(2,1)}, u32[]{:S(2)}, u32[]{:S(2)}) async-start(bf16[4,1024,512]{2,1,0:T(8,128)(2,1)} %bitcast.8), calls=%async_computation | async-start | bytes 8388608 | tf_op jit(solution)/shard_map/all_to_all | solution.py:12
  91.1 185.6 %reduce-scatter.2.cloned.1.call-start = ((), (), s32[]{:S(2)}) async-start(), calls=%async_computation.5 | async-start | bytes 5242880 | tf_op jit(solution)/shard_map/reduce_scatter | solution.py:20
Sparse Core Ops, SparseCore 0:
  10.7 75.5 all-gather.7
  87.8 55.5 all-gather.3
  146.1 72.7 all-gather.5
  233.7 42.9 reduce-scatter.1
where the time goes:
time: 288 us
  waiting for transfers between devices  230 us (80%)
  local copies, waits for them, and re-layouts  17.3 us (6%)
  matrix products  14.7 us (5%)
  between operations  13.8 us (5%)
  other arithmetic  7.31 us (3%)
  starting transfers between devices  5.06 us (2%)
    all_gather x1, waiting for transfers between devices, shards(): gathered = lax.all_gather(down_local, 'fs', axis=0, tiled=True)  73.9 us
    all_gather x1, waiting for transfers between devices, shards(): features = lax.all_gather(tokens, 'tp', axis=1, tiled=True)  52.2 us
    all_gather x1, waiting for transfers between devices, shards(): up_ready = lax.all_gather(up_local, 'fs', axis=0, tiled=True)  50.9 us
    reduce_scatter x1, waiting for transfers between devices, shards(): lax.psum_scatter(partial_value.astype(jnp.bfloat16), 'tp', scatter_dimens...  36.6 us
    all_to_all x1, waiting for transfers between devices, shards(): lax.all_to_all(gathered, 'tp', split_axis=0, concat_axis=1, tiled=True)  15.3 us
    dot_general x1, matrix products, shards(): jnp.dot(hidden, down_ready, preferred_element_type=jnp.float32)  14.7 us
    unnamed x2, local copies, waits for them, and re-layouts  11.1 us
    all_to_all x1, local copies, waits for them, and re-layouts, shards(): lax.all_to_all(gathered, 'tp', split_axis=0, concat_axis=1, tiled=True)  6.21 us
  transfers between devices with their start and end apart: 5, of which 5 were waited for; matrix products, arithmetic and copies ran while one was open for 6% of the time, Pallas kernels for 0%

commit v1 on v0

--- a/solution.py
+++ b/solution.py
@@ -4,11 +4,21 @@
 from jax.sharding import PartitionSpec as P
 
 
+def around_the_ring(array, name, dim):
+    devices = lax.axis_size(name)
+    held, blocks = (array, [array])
+    for _ in range(devices - 1):
+        held = lax.ppermute(held, name, [(i, (i + 1) % devices) for i in range(devices)])
+        blocks.insert(0, held)
+    merged = jnp.concatenate(blocks, axis=dim)
+    return jnp.roll(merged, (lax.axis_index(name) + 1) * array.shape[dim], axis=dim)
+
+
 def shards(tokens, norm_gain, up_master, down_master):
     up_local = (norm_gain[:, None] * up_master).astype(jnp.bfloat16)
     up_ready = lax.all_gather(up_local, "fs", axis=0, tiled=True)
     down_local = down_master.astype(jnp.bfloat16)
-    gathered = lax.all_gather(down_local, "fs", axis=0, tiled=True)
+    gathered = around_the_ring(down_local, "fs", 0)
     down_ready = lax.all_to_all(gathered, "tp", split_axis=0, concat_axis=1, tiled=True)
     features = lax.all_gather(tokens, "tp", axis=1, tiled=True)
     values = features.astype(jnp.float32)

time: 288 us -> 262 us (0.910)
  waiting for transfers between devices: 230 us -> 192 us
  local copies, waits for them, and re-layouts: 17.3 us -> 26.5 us
  starting transfers between devices: 5.06 us -> 8.12 us
    ppermute x0 -> x7, waiting for transfers between devices: none -> 112 us  [around_the_ring(): lax.ppermute(held, name, [(i, (i + 1) % devices) for i in range(devices)])]
    all_gather x1 -> x0, waiting for transfers between devices: 73.9 us -> none  [shards(): gathered = lax.all_gather(down_local, 'fs', axis=0, tiled=True)]
    all_gather x1, waiting for transfers between devices: 52.2 us -> 0.02 us  [shards(): features = lax.all_gather(tokens, 'tp', axis=1, tiled=True)]
    all_gather x1, waiting for transfers between devices: 50.9 us -> 0.01 us  [shards(): up_ready = lax.all_gather(up_local, 'fs', axis=0, tiled=True)]
    all_to_all x1, waiting for transfers between devices: 15.3 us -> 45 us  [shards(): lax.all_to_all(gathered, 'tp', split_axis=0, concat_axis=1, tiled=True)]
    unnamed x2 -> x18, local copies, waits for them, and re-layouts: 11.1 us -> 18 us
    ppermute x0 -> x7, starting transfers between devices: none -> 3.06 us  [around_the_ring(): lax.ppermute(held, name, [(i, (i + 1) % devices) for i in range(devices)])]
  transfers between devices with their start and end apart: 5 -> 11, of which waited for: 5 -> 9; matrix products, arithmetic and copies ran while one was open for 6% -> 11% of each run, Pallas kernels for 0% -> 0%
where the time goes in v1:
time: 262 us
  waiting for transfers between devices  192 us (73%)
  local copies, waits for them, and re-layouts  26.5 us (10%)
  matrix products  14.7 us (6%)
  between operations  13.9 us (5%)
  starting transfers between devices  8.12 us (3%)
  other arithmetic  6.65 us (3%)
    ppermute x7, waiting for transfers between devices, around_the_ring(): lax.ppermute(held, name, [(i, (i + 1) % devices) for i in range(devices)])  112 us
    all_to_all x1, waiting for transfers between devices, shards(): lax.all_to_all(gathered, 'tp', split_axis=0, concat_axis=1, tiled=True)  45 us
    reduce_scatter x1, waiting for transfers between devices, shards(): lax.psum_scatter(partial_value.astype(jnp.bfloat16), 'tp', scatter_dimens...  34 us
    unnamed x18, local copies, waits for them, and re-layouts  18 us
    dot_general x1, matrix products, shards(): jnp.dot(hidden, down_ready, preferred_element_type=jnp.float32)  14.7 us
    all_to_all x1, local copies, waits for them, and re-layouts, shards(): lax.all_to_all(gathered, 'tp', split_axis=0, concat_axis=1, tiled=True)  6.19 us
  transfers between devices with their start and end apart: 11, of which 9 were waited for; matrix products, arithmetic and copies ran while one was open for 11% of the time, Pallas kernels for 0%

profile of v1, /device:TPU:0, one launch (start us, length us, event | category | flops | bytes accessed | tf_op | source)
XLA Modules:
  0.0 261.5 jit_solution(13144986197672626581)
XLA Ops:
  7.2 0.0 copy-start
  7.2 0.0 all-gather.3.cloned.1.call-start
  7.2 0.7 all-gather.3.cloned.1.call-update
  7.9 0.0 all-gather.5.cloned.1.call-start
  8.0 1.3 convert_element_type.22
  9.2 3.0 %collective-permute-start = (bf16[512,512]{1,0:T(8,128)(2,1)S(1)}, bf16[512,512]{1,0:T(8,128)(2,1)S(1)}, u32[]{:S(2)}, u32[]{:S(2)}) collective-permute-start(bf16[512,512]{1,0:T(8,128)(2,1)S(1)} %convert_element_type.22), channel_id=1, source_target_pairs={{0,4},{4,8},{8,12},{12,16},{16,20},{20,24},{24,28},{28,0},{1,5},{5... | collective-permute-start | bytes 1572872 | tf_op jit(solution)/shard_map/ppermute | solution.py:11
  12.3 15.0 %collective-permute-done = bf16[512,512]{1,0:T(8,128)(2,1)S(1)} collective-permute-done((bf16[512,512]{1,0:T(8,128)(2,1)S(1)}, bf16[512,512]{1,0:T(8,128)(2,1)S(1)}, u32[]{:S(2)}, u32[]{:S(2)}) %collective-permute-start) | collective-permute-done | bytes 524320 | tf_op jit(solution)/shard_map/ppermute | solution.py:11
  27.3 0.0 collective-permute-start.1
  27.3 15.8 %collective-permute-done.1 = bf16[512,512]{1,0:T(8,128)(2,1)S(1)} collective-permute-done((bf16[512,512]{1,0:T(8,128)(2,1)S(1)}, bf16[512,512]{1,0:T(8,128)(2,1)S(1)}, u32[]{:S(2)}, u32[]{:S(2)}) %collective-permute-start.1) | collective-permute-done | bytes 524320 | tf_op jit(solution)/shard_map/ppermute | solution.py:11
  43.0 0.0 collective-permute-start.2
  43.0 14.9 %collective-permute-done.2 = bf16[512,512]{1,0:T(8,128)(2,1)S(1)} collective-permute-done((bf16[512,512]{1,0:T(8,128)(2,1)S(1)}, bf16[512,512]{1,0:T(8,128)(2,1)S(1)}, u32[]{:S(2)}, u32[]{:S(2)}) %collective-permute-start.2) | collective-permute-done | bytes 524320 | tf_op jit(solution)/shard_map/ppermute | solution.py:11
  58.0 0.0 collective-permute-start.3
  58.0 14.1 %collective-permute-done.3 = bf16[512,512]{1,0:T(8,128)(2,1)S(1)} collective-permute-done((bf16[512,512]{1,0:T(8,128)(2,1)S(1)}, bf16[512,512]{1,0:T(8,128)(2,1)S(1)}, u32[]{:S(2)}, u32[]{:S(2)}) %collective-permute-start.3) | collective-permute-done | bytes 524320 | tf_op jit(solution)/shard_map/ppermute | solution.py:11
  72.0 0.0 collective-permute-start.4
  72.1 2.1 multiply_convert_fusion.2
  74.2 0.0 all-gather.5.cloned.1.call-update
  74.2 11.2 %collective-permute-done.4 = bf16[512,512]{1,0:T(8,128)(2,1)} collective-permute-done((bf16[512,512]{1,0:T(8,128)(2,1)S(1)}, bf16[512,512]{1,0:T(8,128)(2,1)}, u32[]{:S(2)}, u32[]{:S(2)}) %collective-permute-start.4) | collective-permute-done | bytes 524320 | tf_op jit(solution)/shard_map/ppermute | solution.py:11
  85.4 0.0 collective-permute-start.5
  85.4 27.1 %collective-permute-done.5 = bf16[512,512]{1,0:T(8,128)(2,1)} collective-permute-done((bf16[512,512]{1,0:T(8,128)(2,1)}, bf16[512,512]{1,0:T(8,128)(2,1)}, u32[]{:S(2)}, u32[]{:S(2)}) %collective-permute-start.5) | collective-permute-done | bytes 524320 | tf_op jit(solution)/shard_map/ppermute | solution.py:11
  112.5 0.0 collective-permute-start.6
  112.5 13.8 %collective-permute-done.6 = bf16[512,512]{1,0:T(8,128)(2,1)} collective-permute-done((bf16[512,512]{1,0:T(8,128)(2,1)}, bf16[512,512]{1,0:T(8,128)(2,1)}, u32[]{:S(2)}, u32[]{:S(2)}) %collective-permute-start.6) | collective-permute-done | bytes 524320 | tf_op jit(solution)/shard_map/ppermute | solution.py:11
  126.3 1.1 constant_dynamic-update-slice_fusion.15
  127.4 1.1 constant_dynamic-update-slice_fusion.14
  128.4 1.1 constant_dynamic-update-slice_fusion.13
  129.7 0.0 copy-done
  129.7 0.1 constant_dynamic-update-slice_fusion.8
  129.8 1.1 constant_dynamic-update-slice_fusion.7
  130.9 1.1 constant_dynamic-update-slice_fusion.6
  131.9 1.1 constant_dynamic-update-slice_fusion.5
  133.2 0.1 constant_dynamic-update-slice_fusion
  133.3 2.3 constant_dynamic-slice_fusion
  135.6 4.9 %all-to-all-start = ((bf16[4,1024,512]{2,1,0:T(8,128)(2,1)}), bf16[4,1024,512]{2,1,0:T(8,128)(2,1)}, u32[]{:S(2)}, u32[]{:S(2)}) async-start(bf16[4,1024,512]{2,1,0:T(8,128)(2,1)} %bitcast.7), calls=%async_computation | async-start | bytes 8388608 | tf_op jit(solution)/shard_map/all_to_all | solution.py:22
  140.5 0.0 reduce-scatter.2.cloned.1.call-start
  140.6 0.0 all-gather.3.cloned.1.call-done
  140.6 3.1 %fusion = f32[1024]{0:T(1024)S(1)} fusion(bf16[1024,2048]{1,0:T(8,128)(2,1)} %all-gather.3.cloned.1.call-done), kind=kLoop, calls=%fused_computation.2 | loop fusion | flops 6290432 | bytes 4198400 | tf_op jit(solution)/shard_map/reduce_sum | solution.py:25
  143.7 45.0 %all-to-all-done = bf16[4,1024,512]{2,1,0:T(8,128)(2,1)} async-done(((bf16[4,1024,512]{2,1,0:T(8,128)(2,1)}), bf16[4,1024,512]{2,1,0:T(8,128)(2,1)}, u32[]{:S(2)}, u32[]{:S(2)}) %all-to-all-start) | async-done | bytes 4194336 | tf_op jit(solution)/shard_map/all_to_all | solution.py:22
  188.7 6.2 %copy.7 = bf16[1024,4,512]{0,2,1:T(8,128)(2,1)} copy(bf16[1024,4,512]{2,0,1:T(8,128)(2,1)} %bitcast.1) | data formatting | bytes 8388608 | tf_op jit(solution)/shard_map/all_to_all | solution.py:22
  194.9 0.0 all-gather.5.cloned.1.call-done
  194.9 14.7 %convolution_convert_fusion = bf16[1024,2048]{1,0:T(8,128)(2,1)} fusion(bf16[1024,2048]{0,1:T(8,128)(2,1)} %bitcast.5, bf16[2048,1024]{1,0:T(8,128)(2,1)} %all-gather.5.cloned.1.call-done, bf16[1024,2048]{1,0:T(8,128)(2,1)} %all-gather.3.cloned.1.call-done, f32[1024]{0:T(1024)S(1)} %add_rsqrt_fusion), kind=kOutput, calls=%fused_computation.7 | convolution fusion | flops 8601468928 | bytes 16781312 | tf_op jit(solution)/shard_map/dot_general | solution.py:29
  209.6 0.0 reduce-scatter.2.cloned.1.call-update
  209.7 6.6 %copy.8 = bf16[1024,2048]{1,0:T(8,128)(2,1)} copy(bf16[1024,2048]{0,1:T(8,128)(2,1)} %bitcast.6) | data formatting | bytes 8388608
  216.3 34.0 %reduce-scatter.2.cloned.1.call-done = bf16[1024,512]{1,0:T(8,128)(2,1)} async-done(((bf16[1024,2048]{1,0:T(8,128)(2,1)}), bf16[1024,512]{1,0:T(8,128)(2,1)}) %reduce-scatter.2.cloned.1.call-update) | async-done | bytes 1048592 | tf_op jit(solution)/shard_map/reduce_scatter | solution.py:30
  250.4 4.6 %copy.25 = bf16[2048,1024]{1,0:T(8,128)(2,1)} copy(bf16[2048,1024]{1,0:T(8,128)(2,1)} %all-gather.5.cloned.1.call-done) | data formatting | bytes 8388608
  (9 shorter events, 0.3 us)
Async XLA Ops:
  7.2 122.5 %copy-start = (f32[512,512]{1,0:T(8,128)S(1)}, f32[512,512]{1,0:T(8,128)}, u32[]{:S(2)}) copy-start(f32[512,512]{1,0:T(8,128)} %param.7) | copy-start | bytes 3145732
  7.2 133.4 %all-gather.3.cloned.1.call-start = ((), (), s32[]{:S(2)}) async-start(), calls=%async_computation.2 | async-start | bytes 5242880 | tf_op jit(solution)/shard_map/all_gather | solution.py:23
  7.9 187.0 %all-gather.5.cloned.1.call-start = ((), (), s32[]{:S(2)}) async-start(), calls=%async_computation.3 | async-start | bytes 4718592 | tf_op jit(solution)/shard_map/all_gather | solution.py:19
  9.2 18.0 %collective-permute-start = (bf16[512,512]{1,0:T(8,128)(2,1)S(1)}, bf16[512,512]{1,0:T(8,128)(2,1)S(1)}, u32[]{:S(2)}, u32[]{:S(2)}) collective-permute-start(bf16[512,512]{1,0:T(8,128)(2,1)S(1)} %convert_element_type.22), channel_id=1, source_target_pairs={{0,4},{4,8},{8,12},{12,16},{16,20},{20,24},{24,28},{28,0},{1,5},{5... | collective-permute-start | bytes 1572872 | tf_op jit(solution)/shard_map/ppermute | solution.py:11
  27.3 15.8 %collective-permute-start.1 = (bf16[512,512]{1,0:T(8,128)(2,1)S(1)}, bf16[512,512]{1,0:T(8,128)(2,1)S(1)}, u32[]{:S(2)}, u32[]{:S(2)}) collective-permute-start(bf16[512,512]{1,0:T(8,128)(2,1)S(1)} %collective-permute-done), channel_id=1, source_target_pairs={{0,4},{4,8},{8,12},{12,16},{16,20},{20,24},{24,28},{28,0},{1,5},{5... | collective-permute-start | bytes 1572872 | tf_op jit(solution)/shard_map/ppermute | solution.py:11
  43.0 14.9 %collective-permute-start.2 = (bf16[512,512]{1,0:T(8,128)(2,1)S(1)}, bf16[512,512]{1,0:T(8,128)(2,1)S(1)}, u32[]{:S(2)}, u32[]{:S(2)}) collective-permute-start(bf16[512,512]{1,0:T(8,128)(2,1)S(1)} %collective-permute-done.1), channel_id=1, source_target_pairs={{0,4},{4,8},{8,12},{12,16},{16,20},{20,24},{24,28},{28,0},{1,5},{5... | collective-permute-start | bytes 1572872 | tf_op jit(solution)/shard_map/ppermute | solution.py:11
  58.0 14.1 %collective-permute-start.3 = (bf16[512,512]{1,0:T(8,128)(2,1)S(1)}, bf16[512,512]{1,0:T(8,128)(2,1)S(1)}, u32[]{:S(2)}, u32[]{:S(2)}) collective-permute-start(bf16[512,512]{1,0:T(8,128)(2,1)S(1)} %collective-permute-done.2), channel_id=1, source_target_pairs={{0,4},{4,8},{8,12},{12,16},{16,20},{20,24},{24,28},{28,0},{1,5},{5... | collective-permute-start | bytes 1572872 | tf_op jit(solution)/shard_map/ppermute | solution.py:11
  72.0 13.3 %collective-permute-start.4 = (bf16[512,512]{1,0:T(8,128)(2,1)S(1)}, bf16[512,512]{1,0:T(8,128)(2,1)}, u32[]{:S(2)}, u32[]{:S(2)}) collective-permute-start(bf16[512,512]{1,0:T(8,128)(2,1)S(1)} %collective-permute-done.3), channel_id=1, source_target_pairs={{0,4},{4,8},{8,12},{12,16},{16,20},{20,24},{24,28},{28,0},{1,5},{5... | collective-permute-start | bytes 1572872 | tf_op jit(solution)/shard_map/ppermute | solution.py:11
  85.4 27.1 %collective-permute-start.5 = (bf16[512,512]{1,0:T(8,128)(2,1)}, bf16[512,512]{1,0:T(8,128)(2,1)}, u32[]{:S(2)}, u32[]{:S(2)}) collective-permute-start(bf16[512,512]{1,0:T(8,128)(2,1)} %collective-permute-done.4), channel_id=1, source_target_pairs={{0,4},{4,8},{8,12},{12,16},{16,20},{20,24},{24,28},{28,0},{1,5},{5... | collective-permute-start | bytes 1572872 | tf_op jit(solution)/shard_map/ppermute | solution.py:11
  112.5 13.8 %collective-permute-start.6 = (bf16[512,512]{1,0:T(8,128)(2,1)}, bf16[512,512]{1,0:T(8,128)(2,1)}, u32[]{:S(2)}, u32[]{:S(2)}) collective-permute-start(bf16[512,512]{1,0:T(8,128)(2,1)} %collective-permute-done.5), channel_id=1, source_target_pairs={{0,4},{4,8},{8,12},{12,16},{16,20},{20,24},{24,28},{28,0},{1,5},{5... | collective-permute-start | bytes 1572872 | tf_op jit(solution)/shard_map/ppermute | solution.py:11
  135.6 53.1 %all-to-all-start = ((bf16[4,1024,512]{2,1,0:T(8,128)(2,1)}), bf16[4,1024,512]{2,1,0:T(8,128)(2,1)}, u32[]{:S(2)}, u32[]{:S(2)}) async-start(bf16[4,1024,512]{2,1,0:T(8,128)(2,1)} %bitcast.7), calls=%async_computation | async-start | bytes 8388608 | tf_op jit(solution)/shard_map/all_to_all | solution.py:22
  140.5 109.8 %reduce-scatter.2.cloned.1.call-start = ((), (), s32[]{:S(2)}) async-start(), calls=%async_computation.4 | async-start | bytes 5242880 | tf_op jit(solution)/shard_map/reduce_scatter | solution.py:30
Sparse Core Ops, SparseCore 0:
  9.5 37.1 all-gather.2
  74.3 86.3 all-gather.4
  209.8 40.5 reduce-scatter.1
